TPU v7x, 256 devices: a whole 4x4x8 slice. The times are simulated.
256 devices in a mesh: fs: 32 (over z, y), tp: 8 (over x, core).
Axes of the slice: x: 4, y: 4, z: 8, core: 2. Of those that a mesh axis runs over, the one named last changes fastest.
Arguments:
- tokens: bfloat16 [8192, 2048], P('fs'), may hold values from -6 to 6
- routes: int32 [8192, 6], P('fs'), may hold values from 0 to 31, all different within a row; in each aligned block of 256 rows (0 to 255, 256 to 511, ...) at most 80 rows name the same one
- route_weights: float32 [8192, 6], P('fs'), may hold values from 0.1 to 1
- norm_gain: float32 [2048], P('fs'), may hold values from 0.1 to 1.9
- expert_gate: float32 [32, 2048, 1024], P(None, 'fs', 'tp'), may hold values from -0.125 to 0.125
- expert_up: float32 [32, 2048, 1024], P(None, 'fs', 'tp'), may hold values from -0.125 to 0.125
- expert_down: float32 [32, 2048, 1024], P(None, 'fs', 'tp'), may hold values from -0.1875 to 0.1875
- shared_gate: float32 [2048, 1024], P('fs', 'tp'), may hold values from -0.125 to 0.125
- shared_up: float32 [2048, 1024], P('fs', 'tp'), may hold values from -0.125 to 0.125
- shared_down: float32 [2048, 1024], P('fs', 'tp'), may hold values from -0.1875 to 0.1875
Outputs:
- layer_output: bfloat16 [8192, 2048], P('fs', 'tp')
- sample_gate: bfloat16 [32, 2048, 1024], P('fs', None, 'tp')
- sample_up: bfloat16 [32, 2048, 1024], P('fs', None, 'tp')
- sample_down: bfloat16 [32, 2048, 1024], P('fs', None, 'tp')
- common_gate: bfloat16 [2048, 1024], P(None, 'tp')
- common_up: bfloat16 [2048, 1024], P(None, 'tp')
- common_down: bfloat16 [2048, 1024], P(None, 'tp')
Inputs may be any that keep to these rules, and one draw needn't show every extreme that they name: `routes`: each row names 6 different experts. In each aligned block of 256 rows (the rows of one index of fs) no expert is named by more than 80 rows, a bound that some expert reaches in some blocks.
All inputs are finite; a program needn't handle non-finite values.
Results may differ from a plain program's by a relative error of at most 0.015.
Values may be sent and summed in bfloat16 or wider, within the bound.
A program may use at most 128 MiB of HBM per device.

v0:
```python
import jax
import jax.numpy as jnp
from jax import lax
from jax.sharding import PartitionSpec as P

EPSILON = 1e-06


def normalize(tokens):
    values = tokens.astype(jnp.float32)
    scale = lax.rsqrt(jnp.mean(values * values, axis=-1, keepdims=True) + EPSILON)
    return (values * scale).astype(jnp.bfloat16)


def body(
    tokens,
    routes,
    route_weights,
    norm_gain,
    expert_gate,
    expert_up,
    expert_down,
    shared_gate,
    shared_up,
    shared_down,
):
    bf16, f32 = (jnp.bfloat16, jnp.float32)
    tp_count = lax.axis_size("tp")
    me_tp = lax.axis_index("tp")
    experts = expert_gate.shape[0]
    gain_rows = norm_gain[None, :, None]
    packed = jnp.concatenate(
        [
            (expert_gate * gain_rows).astype(bf16),
            (expert_up * gain_rows).astype(bf16),
            expert_down.astype(bf16),
        ],
        axis=2,
    )
    mine = lax.all_to_all(packed, "fs", split_axis=0, concat_axis=1, tiled=True)
    width = expert_gate.shape[2]
    sample_gate, sample_up, sample_down = (
        mine[:, :, i * width : (i + 1) * width] for i in range(3)
    )
    normed = normalize(tokens)
    tok_rows, depth = normed.shape
    share = tok_rows // tp_count
    hits = routes[:, :, None] == jnp.arange(experts, dtype=jnp.int32)[None, None, :]
    dense = jnp.sum(jnp.where(hits, route_weights[:, :, None], 0.0), axis=1)
    own_rows = lax.dynamic_slice_in_dim(normed, me_tp * share, share, 0)
    own_dense = lax.dynamic_slice_in_dim(dense, me_tp * share, share, 0)
    rows = lax.all_gather(own_rows, "fs", axis=0, tiled=True)
    scales = lax.all_to_all(own_dense.T, "fs", split_axis=0, concat_axis=0, tiled=True)
    scales = scales.reshape(-1, 1)
    shared_packed = jnp.concatenate(
        [
            (shared_gate * norm_gain[:, None]).astype(bf16),
            (shared_up * norm_gain[:, None]).astype(bf16),
            shared_down.astype(bf16),
        ],
        axis=1,
    )
    common = lax.all_gather(shared_packed, "fs", axis=0, tiled=True)
    common_gate, common_up, common_down = (common[:, i * width : (i + 1) * width] for i in range(3))
    sg = jnp.dot(normed, common_gate, preferred_element_type=f32)
    su = jnp.dot(normed, common_up, preferred_element_type=f32)
    sh = (jax.nn.silu(sg) * su).astype(bf16)
    shared_terms = jnp.einsum("th,dh->td", sh, common_down, preferred_element_type=f32).astype(bf16)
    shared_sum = lax.psum_scatter(shared_terms, "tp", scatter_dimension=0, tiled=True)
    whole = lax.all_gather(mine[0], "tp", axis=0, tiled=False)
    total = jnp.zeros((), f32)
    gate = jnp.einsum("rd,bdh->rbh", rows, whole[:, :, :width], preferred_element_type=f32)
    up = jnp.einsum("rd,bdh->rbh", rows, whole[:, :, width : 2 * width], preferred_element_type=f32)
    hidden = (jax.nn.silu(gate) * up).astype(bf16)
    out = jnp.einsum("rbh,bdh->rd", hidden, whole[:, :, 2 * width :], preferred_element_type=f32)
    weighted = (out * scales).astype(bf16)
    routed = lax.psum_scatter(weighted, "fs", scatter_dimension=0, tiled=True)
    final = (routed.astype(f32) + shared_sum.astype(f32)).astype(bf16)
    layer_output = lax.all_to_all(final, "tp", split_axis=1, concat_axis=0, tiled=True)
    return (layer_output, sample_gate, sample_up, sample_down, common_gate, common_up, common_down)


def solution(mesh):
    return jax.shard_map(
        body,
        mesh=mesh,
        in_specs=(
            P("fs", None),
            P("fs", None),
            P("fs", None),
            P("fs"),
            P(None, "fs", "tp"),
            P(None, "fs", "tp"),
            P(None, "fs", "tp"),
            P("fs", "tp"),
            P("fs", "tp"),
            P("fs", "tp"),
        ),
        out_specs=(
            P("fs", "tp"),
            P("fs", None, "tp"),
            P("fs", None, "tp"),
            P("fs", None, "tp"),
            P(None, "tp"),
            P(None, "tp"),
            P(None, "tp"),
        ),
        check_vma=False,
    )
```

profile of v0, /device:TPU:1, one launch (start us, length us, event | category | flops | bytes accessed | tf_op | source)
XLA Modules:
  0.0 528.3 jit_solution(2607383099110861899)
XLA Ops:
  7.2 0.9 convert_element_type.55
  8.1 0.9 multiply_convert_fusion.4
  9.0 0.6 pad_maximum_fusion.1
  9.7 0.0 all-gather.4.cloned.1.call-start
  9.7 1.5 fusion.12
  11.2 1.5 fusion.13
  12.7 0.7 constant_dynamic-slice_fusion.1
  13.5 0.1 convert_element_type.49
  13.6 1.5 multiply_convert_fusion.2
  15.1 0.2 pad_maximum_fusion
  15.3 52.6 %all_to_all.40 = bf16[32,64,384]{2,1,0:T(8,128)(2,1)} all-to-all(bf16[32,64,384]{2,1,0:T(8,128)(2,1)S(1)} %pad_maximum_fusion), channel_id=1, replica_groups=mesh['fs'=32,'tp'=8] {'fs'}, dimensions={0} | all-to-all | bytes 3145728 | tf_op jit(solution)/shard_map/all_to_all | solution.py:40
  68.0 0.1 constant_dynamic-slice_fusion
  68.1 13.8 %all_to_all.41 = f32[32,1,32]{2,1,0:T(1,128)S(1)} all-to-all(f32[32,1,32]{2,1,0:T(1,128)S(1)} %bitcast.35), channel_id=1, replica_groups=mesh['fs'=32,'tp'=8] {'fs'}, dimensions={0} | all-to-all | bytes 8192 | tf_op jit(solution)/shard_map/all_to_all | solution.py:53
  81.9 0.5 broadcast.22
  82.5 0.7 reduce.3
  83.2 0.1 mul.76
  83.2 6.6 %all-gather.8.cloned.1.call-done = bf16[2048,384]{1,0:T(8,128)(2,1)} async-done(((bf16[64,384]{1,0:T(8,128)(2,1)}), bf16[2048,384]{1,0:T(8,128)(2,1)}) %all-gather.8.cloned.1.call-update) | async-done | bytes 1572880 | tf_op jit(solution)/shard_map/all_gather | solution.py:63
  89.8 1.5 fusion.28
  91.3 0.4 fusion.29
  91.7 1.7 convolution_convert_fusion
  93.6 79.8 %all-gather.4.cloned.1.call-done = bf16[1024,2048]{1,0:T(8,128)(2,1)} async-done(((bf16[32,2048]{1,0:T(8,128)(2,1)}), bf16[1024,2048]{1,0:T(8,128)(2,1)}) %all-gather.4.cloned.1.call-update) | async-done | bytes 4194320 | tf_op jit(solution)/shard_map/all_gather | solution.py:52
  173.4 72.4 %all-gather.6.cloned.1.call-done = bf16[8,2048,384]{2,1,0:T(8,128)(2,1)} async-done(((bf16[1,2048,384]{2,1,0:T(8,128)(2,1)}), bf16[8,2048,384]{2,1,0:T(8,128)(2,1)}) %all-gather.6.cloned.1.call-update) | async-done | bytes 12582928 | tf_op jit(solution)/shard_map/all_gather | solution.py:70
  245.8 9.9 %fusion.2 = f32[1024,8,128]{2,0,1:T(8,128)} fusion(bf16[8,2048,384]{2,1,0:T(8,128)(2,1)} %all-gather.6.cloned.1.call-done, bf16[1024,2048]{1,0:T(8,128)(2,1)} %all-gather.4.cloned.1.call-done), kind=kOutput, calls=%fused_computation.3 | convolution fusion | flops 4294967296 | bytes 12582912 | tf_op jit(solution)/shard_map/rd,bdh->rbh/dot_general | solution.py:73
  255.7 15.5 %fusion = bf16[1024,2048]{1,0:T(8,128)(2,1)} fusion(bf16[8,2048,384]{2,1,0:T(8,128)(2,1)} %all-gather.6.cloned.1.call-done, f32[1024]{0:T(1024)S(1)} %mul.76, f32[1024,8,128]{2,0,1:T(8,128)} %fusion.2, bf16[1024,2048]{1,0:T(8,128)(2,1)} %all-gather.4.cloned.1.call-done), kind=kOutput, calls=%fused_computation.1 | convolution fusion | flops 8600420352 | bytes 20975616 | tf_op jit(solution)/shard_map/rbh,bdh->rd/dot_general | solution.py:75
  271.2 9.4 %reduce-scatter.5.cloned.1.call-done = bf16[32,2048]{1,0:T(8,128)(2,1)} async-done(((bf16[256,2048]{1,0:T(8,128)(2,1)}), bf16[32,2048]{1,0:T(8,128)(2,1)}) %reduce-scatter.5.cloned.1.call-update) | async-done | bytes 131088 | tf_op jit(solution)/shard_map/reduce_scatter | solution.py:69
  280.7 223.7 %reduce-scatter.3.cloned.1.call-done = bf16[32,2048]{1,0:T(8,128)(2,1)} async-done(((bf16[1024,2048]{1,0:T(8,128)(2,1)}), bf16[32,2048]{1,0:T(8,128)(2,1)}) %reduce-scatter.3.cloned.1.call-update) | async-done | bytes 131088 | tf_op jit(solution)/shard_map/reduce_scatter | solution.py:77
  504.4 1.0 add_convert_fusion
  505.4 0.7 copy.30
  506.1 9.8 %all-to-all-start.2 = ((bf16[32,8,256]{2,0,1:T(8,128)(2,1)}), bf16[32,8,256]{2,0,1:T(8,128)(2,1)S(1)}, u32[]{:S(2)}, u32[]{:S(2)}) async-start(bf16[32,8,256]{2,0,1:T(8,128)(2,1)} %bitcast.30), calls=%async_computation.4 | async-start | bytes 262144 | tf_op jit(solution)/shard_map/all_to_all | solution.py:79
  515.9 1.2 fusion.27
  517.2 4.0 all-to-all-done.2
  521.2 0.7 copy.32
  (29 shorter events, 0.3 us)
Async XLA Ops:
  7.2 6.4 %copy-start.8 = (f32[64]{0:T(128)S(1)}, f32[64]{0:T(128)}, u32[]{:S(2)}) copy-start(f32[64]{0:T(128)} %param.13) | copy-start | bytes 772
  7.2 6.3 %copy-start.4 = (f32[32,64,128]{2,1,0:T(8,128)S(1)}, f32[32,64,128]{2,1,0:T(8,128)}, u32[]{:S(2)}) copy-start(f32[32,64,128]{2,1,0:T(8,128)} %param.16) | copy-start | bytes 3145732
  7.2 6.4 %copy-start.5 = (f32[32,64,128]{2,1,0:T(8,128)S(1)}, f32[32,64,128]{2,1,0:T(8,128)}, u32[]{:S(2)}) copy-start(f32[32,64,128]{2,1,0:T(8,128)} %param.14) | copy-start | bytes 3145732
  7.2 82.6 %all-gather.8.cloned.1.call-start = ((), (), s32[]{:S(2)}) async-start(), calls=%async_computation.8 | async-start | bytes 1622016 | tf_op jit(solution)/shard_map/all_gather | solution.py:63
  9.7 163.7 %all-gather.4.cloned.1.call-start = ((), (), s32[]{:S(2)}) async-start(), calls=%async_computation.5 | async-start | bytes 4325376 | tf_op jit(solution)/shard_map/all_gather | solution.py:52
  13.4 232.4 %all-gather.6.cloned.1.call-start = ((), (), s32[]{:S(2)}) async-start(), calls=%async_computation.6 | async-start | bytes 14155776 | tf_op jit(solution)/shard_map/all_gather | solution.py:70
  15.1 52.9 %copy-start.6 = (f32[256,6]{0,1:T(8,128)S(1)}, f32[256,6]{0,1:T(8,128)}, u32[]{:S(2)}) copy-start(f32[256,6]{0,1:T(8,128)} %param.12) | copy-start | bytes 18436
  15.1 52.9 %copy-start.7 = (s32[256,6]{0,1:T(8,128)S(1)}, s32[256,6]{0,1:T(8,128)}, u32[]{:S(2)}) copy-start(s32[256,6]{0,1:T(8,128)} %param.11) | copy-start | bytes 18436
  67.9 212.7 %reduce-scatter.5.cloned.1.call-start = ((), (), s32[]{:S(2)}) async-start(), calls=%async_computation.9 | async-start | bytes 1179648 | tf_op jit(solution)/shard_map/reduce_scatter | solution.py:69
  91.3 164.4 %copy-start.1 = (bf16[2048,128]{1,0:T(8,128)(2,1)}, bf16[2048,128]{1,0:T(8,128)(2,1)S(1)}, u32[]{:S(2)}) copy-start(bf16[2048,128]{1,0:T(8,128)(2,1)S(1)} %get-tuple-element.30) | copy-start | bytes 1572868
  91.3 164.4 %copy-start.2 = (bf16[2048,128]{1,0:T(8,128)(2,1)}, bf16[2048,128]{1,0:T(8,128)(2,1)S(1)}, u32[]{:S(2)}) copy-start(bf16[2048,128]{1,0:T(8,128)(2,1)S(1)} %get-tuple-element.29) | copy-start | bytes 1572868
  91.3 164.4 %copy-start.3 = (bf16[2048,128]{1,0:T(8,128)(2,1)}, bf16[2048,128]{1,0:T(8,128)(2,1)S(1)}, u32[]{:S(2)}) copy-start(bf16[2048,128]{1,0:T(8,128)(2,1)S(1)} %get-tuple-element.28) | copy-start | bytes 1572868
  93.5 410.9 %reduce-scatter.3.cloned.1.call-start = ((), (), s32[]{:S(2)}) async-start(), calls=%async_computation.7 | async-start | bytes 4325376 | tf_op jit(solution)/shard_map/reduce_scatter | solution.py:77
  271.2 244.7 %copy-start = (bf16[32,64,384]{2,1,0:T(8,128)(2,1)S(1)}, bf16[32,64,384]{2,1,0:T(8,128)(2,1)}, u32[]{:S(2)}) copy-start(bf16[32,64,384]{2,1,0:T(8,128)(2,1)} %all_to_all.40) | copy-start | bytes 4718596
  506.1 15.1 %all-to-all-start.2 = ((bf16[32,8,256]{2,0,1:T(8,128)(2,1)}), bf16[32,8,256]{2,0,1:T(8,128)(2,1)S(1)}, u32[]{:S(2)}, u32[]{:S(2)}) async-start(bf16[32,8,256]{2,0,1:T(8,128)(2,1)} %bitcast.30), calls=%async_computation.4 | async-start | bytes 262144 | tf_op jit(solution)/shard_map/all_to_all | solution.py:79
Sparse Core Ops, SparseCore 0:
  11.2 78.6 all-gather.7
  93.0 80.3 all-gather.3
  175.2 70.5 all-gather.5
  248.2 32.4 reduce-scatter.4
  284.4 219.9 reduce-scatter.2
where the time goes:
time: 529 us; the launch traced here: 528 us
  waiting for transfers between devices  396 us (75%)
  blocking collectives  66.4 us (13%)
  matrix products  27.6 us (5%)
  between operations  14 us (3%)
  starting transfers between devices  10 us (2%)
  other arithmetic  8.9 us (2%)
  local copies, waits for them, and re-layouts  5.4 us (1%)
    reduce_scatter x1, waiting for transfers between devices, body(): routed = lax.psum_scatter(weighted, 'fs', scatter_dimension=0, tiled=True)  224 us
    all_gather x1, waiting for transfers between devices, body(): rows = lax.all_gather(own_rows, 'fs', axis=0, tiled=True)  79.8 us
    all_gather x1, waiting for transfers between devices, body(): whole = lax.all_gather(mine[0], 'tp', axis=0, tiled=False)  72.4 us
    all_to_all x1, blocking collectives, body(): mine = lax.all_to_all(packed, 'fs', split_axis=0, concat_axis=1, tiled=True)  52.6 us
    dot_general x1, matrix products, body(): jnp.einsum('rbh,bdh->rd', hidden, whole[:, :, 2 * width:], preferred_elem...  15.5 us
    all_to_all x1, blocking collectives, body(): lax.all_to_all(own_dense.T, 'fs', split_axis=0, concat_axis=0, tiled=True)  13.8 us
  transfers between devices with their start and end apart: 6, of which 6 were waited for; matrix products, arithmetic and copies ran while one was open for 7% of the time, Pallas kernels for 0%

commit v1 on v0

--- a/solution.py
+++ b/solution.py
@@ -4,6 +4,14 @@
 from jax.sharding import PartitionSpec as P
 
 EPSILON = 1e-06
+
+
+def tiled_gather(value, axis, dim):
+    size = lax.axis_size(axis)
+    repeats = [size if d == dim else 1 for d in range(value.ndim)]
+    return lax.all_to_all(
+        jnp.tile(value, repeats), axis, split_axis=dim, concat_axis=dim, tiled=True
+    )
 
 
 def normalize(tokens):
@@ -49,7 +57,7 @@
     dense = jnp.sum(jnp.where(hits, route_weights[:, :, None], 0.0), axis=1)
     own_rows = lax.dynamic_slice_in_dim(normed, me_tp * share, share, 0)
     own_dense = lax.dynamic_slice_in_dim(dense, me_tp * share, share, 0)
-    rows = lax.all_gather(own_rows, "fs", axis=0, tiled=True)
+    rows = tiled_gather(own_rows, "fs", 0)
     scales = lax.all_to_all(own_dense.T, "fs", split_axis=0, concat_axis=0, tiled=True)
     scales = scales.reshape(-1, 1)
     shared_packed = jnp.concatenate(

time: 529 us -> 468 us (0.88)
  blocking collectives: 66.4 us -> 0 us
  starting transfers between devices: 10 us -> 32.9 us
  waiting for transfers between devices: 396 us -> 376 us
    all_to_all x0 -> x3, waiting for transfers between devices: none -> 119 us  [the longest x1 72.5 us: tiled_gather(): lax.all_to_all(jnp.tile(value, repeats), axis, split_axis=dim, concat_axi...]
    all_gather x1 -> x0, waiting for transfers between devices: 79.8 us -> none  [body(): rows = lax.all_gather(own_rows, 'fs', axis=0, tiled=True)]
    all_gather x1, waiting for transfers between devices: 72.4 us -> 0.87 us  [body(): whole = lax.all_gather(mine[0], 'tp', axis=0, tiled=False)]
    all_to_all x2 -> x0, blocking collectives: 66.4 us -> none  [the longest x1 52.6 us: body(): mine = lax.all_to_all(packed, 'fs', split_axis=0, concat_axis=1, tiled=True)]
    all_to_all x0 -> x3, starting transfers between devices: none -> 22.9 us  [the longest x1 12 us: body(): mine = lax.all_to_all(packed, 'fs', split_axis=0, concat_axis=1, tiled=True)]
    all_gather x1, waiting for transfers between devices: 6.59 us -> 19.5 us  [body(): common = lax.all_gather(shared_packed, 'fs', axis=0, tiled=True)]
  transfers between devices with their start and end apart: 6 -> 8, of which waited for: 6 -> 8; matrix products, arithmetic and copies ran while one was open for 7% -> 8% of each run, Pallas kernels for 0% -> 0%
where the time goes in v1:
time: 468 us; the launch traced here: 467 us
  waiting for transfers between devices  376 us (80%)
  starting transfers between devices  32.9 us (7%)
  matrix products  27.6 us (6%)
  between operations  14 us (3%)
  local copies, waits for them, and re-layouts  9.04 us (2%)
  other arithmetic  7.57 us (2%)
    reduce_scatter x1, waiting for transfers between devices, body(): routed = lax.psum_scatter(weighted, 'fs', scatter_dimension=0, tiled=True)  224 us
    all_to_all x1, waiting for transfers between devices, tiled_gather(): lax.all_to_all(jnp.tile(value, repeats), axis, split_axis=dim, concat_axi...  72.5 us
    all_to_all x1, waiting for transfers between devices, body(): mine = lax.all_to_all(packed, 'fs', split_axis=0, concat_axis=1, tiled=True)  38.1 us
    all_gather x1, waiting for transfers between devices, body(): common = lax.all_gather(shared_packed, 'fs', axis=0, tiled=True)  19.5 us
    dot_general x1, matrix products, body(): jnp.einsum('rbh,bdh->rd', hidden, whole[:, :, 2 * width:], preferred_elem...  15.5 us
    all_to_all x1, starting transfers between devices, body(): mine = lax.all_to_all(packed, 'fs', split_axis=0, concat_axis=1, tiled=True)  12 us
    dot_general x1, matrix products, body(): jnp.einsum('rd,bdh->rbh', rows, whole[:, :, width:2 * width], preferred_e...  9.94 us
    all_to_all x1, starting transfers between devices, body(): lax.all_to_all(final, 'tp', split_axis=1, concat_axis=0, tiled=True)  9.78 us
  transfers between devices with their start and end apart: 8, of which 8 were waited for; matrix products, arithmetic and copies ran while one was open for 8% of the time, Pallas kernels for 0%

profile of v1, /device:TPU:1, one launch (start us, length us, event | category | flops | bytes accessed | tf_op | source)
XLA Modules:
  0.0 467.5 jit_solution(15459333582352861408)
XLA Ops:
  7.2 1.3 convert_element_type.49
  8.5 1.9 multiply_convert_fusion.2
  10.5 1.4 pad_maximum_fusion
  11.9 12.0 %all-to-all-start.1 = ((bf16[32,64,384]{2,1,0:T(8,128)(2,1)}), bf16[32,64,384]{2,1,0:T(8,128)(2,1)S(1)}, u32[]{:S(2)}, u32[]{:S(2)}) async-start(bf16[32,64,384]{2,1,0:T(8,128)(2,1)} %pad_maximum_fusion), calls=%async_computation.1 | async-start | bytes 3145728 | tf_op jit(solution)/shard_map/all_to_all | solution.py:48
  24.1 0.6 pad_maximum_fusion.1
  24.8 38.1 %all-to-all-done.1 = bf16[32,64,384]{2,1,0:T(8,128)(2,1)S(1)} async-done(((bf16[32,64,384]{2,1,0:T(8,128)(2,1)}), bf16[32,64,384]{2,1,0:T(8,128)(2,1)S(1)}, u32[]{:S(2)}, u32[]{:S(2)}) %all-to-all-start.1) | async-done | bytes 1572896 | tf_op jit(solution)/shard_map/all_to_all | solution.py:48
  62.9 1.2 copy-done
  64.2 0.7 constant_dynamic-slice_fusion
  64.9 6.0 %all-to-all-start.2 = ((f32[32,1,32]{2,1,0:T(1,128)}), f32[32,1,32]{2,1,0:T(1,128)S(1)}, u32[]{:S(2)}, u32[]{:S(2)}) async-start(f32[32,1,32]{2,1,0:T(1,128)} %bitcast.7), calls=%async_computation.2 | async-start | bytes 32768 | tf_op jit(solution)/shard_map/all_to_all | solution.py:61
  71.0 0.3 fusion.8
  71.3 0.2 fusion.9
  71.5 8.0 %all-to-all-done.2 = f32[32,1,32]{2,1,0:T(1,128)S(1)} async-done(((f32[32,1,32]{2,1,0:T(1,128)}), f32[32,1,32]{2,1,0:T(1,128)S(1)}, u32[]{:S(2)}, u32[]{:S(2)}) %all-to-all-start.2) | async-done | bytes 4128 | tf_op jit(solution)/shard_map/all_to_all | solution.py:61
  79.5 2.5 tile.2
  82.0 4.9 %all-to-all-start = ((bf16[32,32,2048]{2,1,0:T(8,128)(2,1)}), bf16[32,32,2048]{2,1,0:T(8,128)(2,1)}, u32[]{:S(2)}, u32[]{:S(2)}) async-start(bf16[32,32,2048]{2,1,0:T(8,128)(2,1)} %tile.2), calls=%async_computation | async-start | bytes 8388608 | tf_op jit(solution)/shard_map/all_to_all | solution.py:12
  86.9 0.5 broadcast.25
  87.4 0.7 reduce.3
  88.2 19.5 %all-gather.5.cloned.1.call-done = bf16[2048,384]{1,0:T(8,128)(2,1)} async-done(((bf16[64,384]{1,0:T(8,128)(2,1)}), bf16[2048,384]{1,0:T(8,128)(2,1)}) %all-gather.5.cloned.1.call-update) | async-done | bytes 1572880 | tf_op jit(solution)/shard_map/all_gather | solution.py:71
  107.7 1.5 fusion.22
  109.2 0.4 fusion.23
  109.6 1.7 convolution_convert_fusion
  111.5 72.5 %all-to-all-done = bf16[32,32,2048]{2,1,0:T(8,128)(2,1)} async-done(((bf16[32,32,2048]{2,1,0:T(8,128)(2,1)}), bf16[32,32,2048]{2,1,0:T(8,128)(2,1)}, u32[]{:S(2)}, u32[]{:S(2)}) %all-to-all-start) | async-done | bytes 4194336 | tf_op jit(solution)/shard_map/all_to_all | solution.py:12
  184.0 0.9 all-gather.3.cloned.1.call-done
  184.8 9.9 %fusion.2 = f32[1024,8,128]{2,0,1:T(8,128)} fusion(bf16[1024,2048,1]{1,0,2:T(8,128)(2,1)} %bitcast.1, bf16[8,2048,384]{2,1,0:T(8,128)(2,1)} %all-gather.3.cloned.1.call-done), kind=kOutput, calls=%fused_computation.3 | convolution fusion | flops 4294967296 | bytes 12582912 | tf_op jit(solution)/shard_map/rd,bdh->rbh/dot_general | solution.py:81
  194.8 15.5 %fusion = bf16[1024,2048]{1,0:T(8,128)(2,1)} fusion(bf16[8,2048,384]{2,1,0:T(8,128)(2,1)} %all-gather.3.cloned.1.call-done, f32[1024]{0:T(1024)S(1)} %mul.76, f32[1024,8,128]{2,0,1:T(8,128)} %fusion.2, bf16[1024,2048,1]{1,0,2:T(8,128)(2,1)} %bitcast.1), kind=kOutput, calls=%fused_computation.1 | convolution fusion | flops 8600420352 | bytes 20975616 | tf_op jit(solution)/shard_map/rbh,bdh->rd/dot_general | solution.py:83
  210.3 9.6 %reduce-scatter.5.cloned.1.call-done = bf16[32,2048]{1,0:T(8,128)(2,1)} async-done(((bf16[256,2048]{1,0:T(8,128)(2,1)}), bf16[32,2048]{1,0:T(8,128)(2,1)}) %reduce-scatter.5.cloned.1.call-update) | async-done | bytes 131088 | tf_op jit(solution)/shard_map/reduce_scatter | solution.py:77
  219.9 223.7 %reduce-scatter.3.cloned.1.call-done = bf16[32,2048]{1,0:T(8,128)(2,1)} async-done(((bf16[1024,2048]{1,0:T(8,128)(2,1)}), bf16[32,2048]{1,0:T(8,128)(2,1)}) %reduce-scatter.3.cloned.1.call-update) | async-done | bytes 131088 | tf_op jit(solution)/shard_map/reduce_scatter | solution.py:85
  443.6 1.0 add_convert_fusion
  444.6 0.7 copy.30
  445.3 9.8 %all-to-all-start.3 = ((bf16[32,8,256]{2,0,1:T(8,128)(2,1)}), bf16[32,8,256]{2,0,1:T(8,128)(2,1)S(1)}, u32[]{:S(2)}, u32[]{:S(2)}) async-start(bf16[32,8,256]{2,0,1:T(8,128)(2,1)} %bitcast.26), calls=%async_computation.5 | async-start | bytes 262144 | tf_op jit(solution)/shard_map/all_to_all | solution.py:87
  455.0 1.2 fusion.21
  456.3 4.0 all-to-all-done.3
  460.3 0.7 copy.32
  (37 shorter events, 0.5 us)
Async XLA Ops:
  8.5 15.5 %copy-start.8 = (f32[64,128]{1,0:T(8,128)S(1)}, f32[64,128]{1,0:T(8,128)}, u32[]{:S(2)}) copy-start(f32[64,128]{1,0:T(8,128)} %param.19) | copy-start | bytes 98308
  8.5 15.5 %copy-start.6 = (f32[64,128]{1,0:T(8,128)S(1)}, f32[64,128]{1,0:T(8,128)}, u32[]{:S(2)}) copy-start(f32[64,128]{1,0:T(8,128)} %param.17) | copy-start | bytes 98308
  8.5 15.5 %copy-start.7 = (f32[64,128]{1,0:T(8,128)S(1)}, f32[64,128]{1,0:T(8,128)}, u32[]{:S(2)}) copy-start(f32[64,128]{1,0:T(8,128)} %param.18) | copy-start | bytes 98308
  8.5 15.5 %copy-start.11 = (f32[64]{0:T(128)S(1)}, f32[64]{0:T(128)}, u32[]{:S(2)}) copy-start(f32[64]{0:T(128)} %param.13) | copy-start | bytes 772
  10.4 53.7 %copy-start.9 = (f32[256,6]{0,1:T(8,128)S(1)}, f32[256,6]{0,1:T(8,128)}, u32[]{:S(2)}) copy-start(f32[256,6]{0,1:T(8,128)} %param.12) | copy-start | bytes 18436
  10.5 53.7 %copy-start.10 = (s32[256,6]{0,1:T(8,128)S(1)}, s32[256,6]{0,1:T(8,128)}, u32[]{:S(2)}) copy-start(s32[256,6]{0,1:T(8,128)} %param.11) | copy-start | bytes 18436
  10.5 60.5 %copy-start.2 = (bf16[256,2048]{1,0:T(8,128)(2,1)S(1)}, bf16[256,2048]{1,0:T(8,128)(2,1)}, u32[]{:S(2)}) copy-start(bf16[256,2048]{1,0:T(8,128)(2,1)} %param.10) | copy-start | bytes 3145732
  11.9 51.1 %all-to-all-start.1 = ((bf16[32,64,384]{2,1,0:T(8,128)(2,1)}), bf16[32,64,384]{2,1,0:T(8,128)(2,1)S(1)}, u32[]{:S(2)}, u32[]{:S(2)}) async-start(bf16[32,64,384]{2,1,0:T(8,128)(2,1)} %pad_maximum_fusion), calls=%async_computation.1 | async-start | bytes 3145728 | tf_op jit(solution)/shard_map/all_to_all | solution.py:48
  23.9 83.8 %all-gather.5.cloned.1.call-start = ((), (), s32[]{:S(2)}) async-start(), calls=%async_computation.8 | async-start | bytes 1622016 | tf_op jit(solution)/shard_map/all_gather | solution.py:71
  24.7 160.1 %all-gather.3.cloned.1.call-start = ((), (), s32[]{:S(2)}) async-start(), calls=%async_computation.6 | async-start | bytes 14155776 | tf_op jit(solution)/shard_map/all_gather | solution.py:78
  62.9 1.2 copy-start
  64.9 14.6 %all-to-all-start.2 = ((f32[32,1,32]{2,1,0:T(1,128)}), f32[32,1,32]{2,1,0:T(1,128)S(1)}, u32[]{:S(2)}, u32[]{:S(2)}) async-start(f32[32,1,32]{2,1,0:T(1,128)} %bitcast.7), calls=%async_computation.2 | async-start | bytes 32768 | tf_op jit(solution)/shard_map/all_to_all | solution.py:61
  82.0 102.0 %all-to-all-start = ((bf16[32,32,2048]{2,1,0:T(8,128)(2,1)}), bf16[32,32,2048]{2,1,0:T(8,128)(2,1)}, u32[]{:S(2)}, u32[]{:S(2)}) async-start(bf16[32,32,2048]{2,1,0:T(8,128)(2,1)} %tile.2), calls=%async_computation | async-start | bytes 8388608 | tf_op jit(solution)/shard_map/all_to_all | solution.py:12
  86.8 133.0 %reduce-scatter.5.cloned.1.call-start = ((), (), s32[]{:S(2)}) async-start(), calls=%async_computation.9 | async-start | bytes 1179648 | tf_op jit(solution)/shard_map/reduce_scatter | solution.py:77
  109.2 85.6 %copy-start.3 = (bf16[2048,128]{1,0:T(8,128)(2,1)}, bf16[2048,128]{1,0:T(8,128)(2,1)S(1)}, u32[]{:S(2)}) copy-start(bf16[2048,128]{1,0:T(8,128)(2,1)S(1)} %get-tuple-element.30) | copy-start | bytes 1572868
  109.2 85.6 %copy-start.4 = (bf16[2048,128]{1,0:T(8,128)(2,1)}, bf16[2048,128]{1,0:T(8,128)(2,1)S(1)}, u32[]{:S(2)}) copy-start(bf16[2048,128]{1,0:T(8,128)(2,1)S(1)} %get-tuple-element.29) | copy-start | bytes 1572868
  109.2 85.6 %copy-start.5 = (bf16[2048,128]{1,0:T(8,128)(2,1)}, bf16[2048,128]{1,0:T(8,128)(2,1)S(1)}, u32[]{:S(2)}) copy-start(bf16[2048,128]{1,0:T(8,128)(2,1)S(1)} %get-tuple-element.28) | copy-start | bytes 1572868
  111.4 332.2 %reduce-scatter.3.cloned.1.call-start = ((), (), s32[]{:S(2)}) async-start(), calls=%async_computation.7 | async-start | bytes 4325376 | tf_op jit(solution)/shard_map/reduce_scatter | solution.py:85
  210.3 244.8 %copy-start.1 = (bf16[32,64,384]{2,1,0:T(8,128)(2,1)S(1)}, bf16[32,64,384]{2,1,0:T(8,128)(2,1)}, u32[]{:S(2)}) copy-start(bf16[32,64,384]{2,1,0:T(8,128)(2,1)} %copy-done) | copy-start | bytes 4718596
  445.3 15.0 %all-to-all-start.3 = ((bf16[32,8,256]{2,0,1:T(8,128)(2,1)}), bf16[32,8,256]{2,0,1:T(8,128)(2,1)S(1)}, u32[]{:S(2)}, u32[]{:S(2)}) async-start(bf16[32,8,256]{2,0,1:T(8,128)(2,1)} %bitcast.26), calls=%async_computation.5 | async-start | bytes 262144 | tf_op jit(solution)/shard_map/all_to_all | solution.py:87
Sparse Core Ops, SparseCore 0:
  27.9 79.7 all-gather.4
  109.5 75.2 all-gather.2
  187.4 32.4 reduce-scatter.4
  223.6 219.9 reduce-scatter.2
